TPU v7x, 32 devices: a whole 2x2x4 slice. The times are simulated.
32 devices in a mesh: sp: 4 (over z), fs: 4 (over y, core), tp: 2 (over x).
Axes of the slice: x: 2, y: 2, z: 4, core: 2. Of those that a mesh axis runs over, the one named last changes fastest.
Arguments:
- input_layer_rows: bfloat16 [4, 1024, 2048], P('fs', 'sp'), may hold values from -6 to 6
- input_norm_gain: float32 [2048], replicated, may hold values from 0.1 to 1.9
- query_weight_attention: bfloat16 [2048, 1024], P(('sp', 'fs'), 'tp'), may hold values from -0.125 to 0.125
- key_weight_attention: bfloat16 [2048, 1024], P(('sp', 'fs'), 'tp'), may hold values from -0.125 to 0.125
- value_weight_attention: bfloat16 [2048, 1024], P(('sp', 'fs'), 'tp'), may hold values from -0.125 to 0.125
- query_weight_recurrent: bfloat16 [2048, 1024], P(('sp', 'fs'), 'tp'), may hold values from -0.125 to 0.125
- forget_weight_recurrent: bfloat16 [2048, 1024], P(('sp', 'fs'), 'tp'), may hold values from -0.125 to 0.125
- value_weight_recurrent: bfloat16 [2048, 1024], P(('sp', 'fs'), 'tp'), may hold values from -0.125 to 0.125
- gate_weight_recurrent: bfloat16 [2048, 1024], P(('sp', 'fs'), 'tp'), may hold values from -0.125 to 0.125
- output_weight_attention: bfloat16 [2048, 1024], P(('sp', 'fs'), 'tp'), may hold values from -0.125 to 0.125
- emitted_projection_linear_scan: bfloat16 [2048, 1024], P(('sp', 'fs'), 'tp'), may hold values from -0.125 to 0.125
- score_offset: float32 [8], P('tp'), as said below
- attention_norm_gain: float32 [1024], P('tp'), may hold values from 0.1 to 1.9
- recurrence_norm_gain: float32 [1024], P('tp'), may hold values from 0.1 to 1.9
- forget_floor: float32 [1024], P('tp'), may hold values from 0.1 to 0.5
- forget_offset: float32 [1024], P('tp'), as said below
- extra_log_decay: float32 [4, 1024, 1024], P('fs', 'sp', 'tp')
Outputs:
- layer_out: bfloat16 [4, 1024, 2048], P('fs', ('sp', 'tp'))
- row_log_total: float32 [4, 8, 1024], P('fs', 'tp', 'sp')
Inputs may be any that keep to these rules, and one draw needn't show every extreme that they name: `score_offset`: each head's offset lies between -ln(1024) - 2 and -ln(1024) + 0.5. `forget_offset`: each channel's offset lies between ln(256) - 3 and ln(1024) + 0.6.
All inputs are finite; a program needn't handle non-finite values.
Results may differ from a plain program's by a relative error of at most 0.015.
Values may be sent and summed in bfloat16 or wider, within the bound.
A program may use at most 64 MiB of HBM per device.

v0:
```python
import jax
import jax.numpy as jnp
from jax import lax
from jax.sharding import PartitionSpec as P

HEAD = 128
BLOCK = 64
epsilon = 1e-06
log_floor = 0.05


def entering(shard, axis, combine, identity):
    size, index = (lax.axis_size(axis), lax.axis_index(axis))
    everything = jax.tree.map(
        lambda part, kind: lax.all_gather(part.astype(kind), axis),
        shard,
        (jnp.bfloat16, jnp.bfloat16),
    )
    start = jax.tree.map(
        lambda part, zero: jnp.broadcast_to(jnp.asarray(zero, part.dtype), part.shape),
        shard,
        identity,
    )

    def hop(k, before):
        reached = k < index
        new = combine(
            before, jax.tree.map(lambda part, own: part[k].astype(own.dtype), everything, shard)
        )
        return jax.tree.map(lambda a, b: jnp.where(reached, a, b), new, before)

    return lax.fori_loop(0, size, hop, start)


def head_norm(values, gain):
    square_mean = jnp.mean(values * values, axis=-1, keepdims=True)
    return values * lax.rsqrt(square_mean + epsilon) * gain


def recurrence_block(memory_matrix, inputs):
    query_slice, decay_part, key_slice, value_slice = inputs
    highest_score = lax.Precision.HIGHEST
    length = decay_part.shape[0]
    running_total = jnp.cumsum(decay_part, axis=0)
    causal = (
        lax.broadcasted_iota(jnp.int32, (length, length), 0)
        >= lax.broadcasted_iota(jnp.int32, (length, length), 1)
    )[:, :, None, None]
    relative = jnp.where(causal, running_total[:, None] - running_total[None, :], -jnp.inf)
    pairwise = jnp.sum(query_slice[:, None] * key_slice[None, :] * jnp.exp(relative), axis=-1)
    inner_part = jnp.einsum("tsh,shv->thv", pairwise, value_slice, precision=highest_score)
    carried_state = jnp.einsum(
        "fby,bym->fbm", query_slice * jnp.exp(running_total), memory_matrix, precision=highest_score
    )
    final_total = running_total[-1]
    updated_state = jnp.exp(final_total)[:, :, None] * memory_matrix + jnp.einsum(
        "rxc,rxa->xca",
        key_slice * jnp.exp(final_total[None] - running_total),
        value_slice,
        precision=highest_score,
    )
    return (updated_state, inner_part + carried_state)


def stick_piece(queries, shifts, weighted, keep_total, key_value, is_own, is_valid):
    scores = (
        jnp.einsum("thd,shd->hts", queries, key_value[0], preferred_element_type=jnp.float32)
        * HEAD ** (-0.5)
        + shifts[:, None, None]
    )
    logarithmic_retention = jax.nn.log_sigmoid(-scores)
    if is_own:
        rows_here = scores.shape[1]
        strict = lax.broadcasted_iota(jnp.int32, (rows_here, rows_here), 0) > lax.broadcasted_iota(
            jnp.int32, (rows_here, rows_here), 1
        )
        logarithmic_retention = jnp.where(strict, logarithmic_retention, 0.0)
    suffix = lax.cumsum(logarithmic_retention, axis=2, reverse=True) - logarithmic_retention
    log_weight = jax.nn.log_sigmoid(scores) + suffix + keep_total[:, :, None]
    if is_own:
        log_weight = jnp.where(strict, log_weight, -jnp.inf)
    weights = jnp.where(is_valid, jnp.exp(log_weight), 0.0).astype(jnp.bfloat16)
    weighted = weighted + jnp.einsum(
        "hts,shd->thd", weights, key_value[1], preferred_element_type=jnp.float32
    )
    keep_total = keep_total + jnp.where(is_valid, jnp.sum(logarithmic_retention, axis=2), 0.0)
    return (weighted, keep_total)


def contract_rows(rows_in, weight):
    return lax.dot_general(
        rows_in, weight, (((1,), (1,)), ((), ())), preferred_element_type=jnp.float32
    )


def on_device(
    input_layer_rows,
    input_norm_gain,
    query_weight_attention,
    key_weight_attention,
    value_weight_attention,
    query_weight_recurrent,
    forget_weight_recurrent,
    value_weight_recurrent,
    gate_weight_recurrent,
    output_weight_attention,
    emitted_projection_linear_scan,
    score_offset,
    attention_norm_gain,
    recurrence_norm_gain,
    forget_floor,
    forget_offset,
    extra_log_decay,
):
    values = input_layer_rows[0].astype(jnp.float32)
    square_mean = jnp.mean(values * values, axis=-1, keepdims=True)
    normed = (values * lax.rsqrt(square_mean + epsilon) * input_norm_gain).astype(jnp.bfloat16)
    tokens = normed.shape[0]
    weights_in = (
        query_weight_attention,
        key_weight_attention,
        value_weight_attention,
        query_weight_recurrent,
        forget_weight_recurrent,
        value_weight_recurrent,
        gate_weight_recurrent,
    )
    pieces = (
        lax.all_gather(weights_in[0], ("sp", "fs"), axis=0, tiled=True),
        lax.all_gather(weights_in[1], ("sp", "fs"), axis=0, tiled=True),
        lax.all_gather(weights_in[2], ("sp", "fs"), axis=0, tiled=True),
        lax.all_gather(weights_in[3], ("sp", "fs"), axis=0, tiled=True),
        lax.all_gather(weights_in[4], ("sp", "fs"), axis=0, tiled=True),
        lax.all_gather(weights_in[5], ("sp", "fs"), axis=0, tiled=True),
        lax.all_gather(weights_in[6], ("sp", "fs"), axis=0, tiled=True),
    )
    projected = tuple(
        (jnp.dot(normed, weight, preferred_element_type=jnp.float32) for weight in pieces)
    )
    query_a, key_a, value_a, query_b, forget_b, input_b, gate_b = [
        column_block.astype(jnp.bfloat16) for column_block in projected
    ]
    out_a, out_b = (
        lax.all_gather(output_weight_attention, ("sp", "fs"), axis=0, tiled=True),
        lax.all_gather(emitted_projection_linear_scan, ("sp", "fs"), axis=0, tiled=True),
    )
    head_count = query_a.shape[1] // HEAD
    queries = query_a.reshape(tokens, head_count, HEAD)
    key_value = jnp.stack(
        [key_a.reshape(tokens, head_count, HEAD), value_a.reshape(tokens, head_count, HEAD)]
    )
    weighted = jnp.zeros((tokens, head_count, HEAD), jnp.float32)
    keep_total = jnp.zeros((head_count, tokens), jnp.float32)
    weighted, keep_total = stick_piece(
        queries, score_offset, weighted, keep_total, key_value, True, True
    )
    position = lax.axis_index("sp")
    seq_devices = lax.axis_size("sp")
    gathered = lax.all_gather(key_value, "sp", axis=1, tiled=True)

    def gathered_turn(turn_index, carried_state):
        weighted_now, keep_now = carried_state
        source = jnp.maximum(position - turn_index, 0) * tokens
        piece_pair = lax.dynamic_slice_in_dim(gathered, source, tokens, 1)
        return stick_piece(
            queries, score_offset, weighted_now, keep_now, piece_pair, False, position >= turn_index
        )

    weighted, keep_total = lax.fori_loop(1, seq_devices, gathered_turn, (weighted, keep_total))
    row_log_total = jnp.log(jnp.maximum(-jnp.expm1(keep_total), log_floor))[None]
    mixed_a = (
        head_norm(weighted, attention_norm_gain.reshape(head_count, HEAD))
        .reshape(tokens, head_count * HEAD)
        .astype(jnp.bfloat16)
    )
    forget_logits = forget_b.astype(jnp.float32) + forget_offset
    forget_log_value = (
        jnp.logaddexp(
            jnp.log(forget_floor), jnp.log1p(-forget_floor) + jax.nn.log_sigmoid(forget_logits)
        )
        + extra_log_decay[0]
    )
    key_in = (1.0 - forget_floor) * jax.nn.sigmoid(-forget_logits)
    query_rows_input = jax.nn.silu(query_b.astype(jnp.float32)).reshape(tokens, head_count, HEAD)
    value_in = input_b.astype(jnp.float32)
    fading_channel_groups = forget_log_value.reshape(tokens, head_count, HEAD)
    shaped = tuple(
        (
            array_in.reshape(tokens // BLOCK, BLOCK, head_count, HEAD)
            for array_in in (query_rows_input, forget_log_value, key_in, value_in)
        )
    )
    empty_state = jnp.zeros((head_count, HEAD, HEAD), jnp.float32)
    nearby_hidden_vector, local_out = lax.scan(recurrence_block, empty_state, shaped)
    local_out = local_out.reshape(tokens, head_count, HEAD)
    through = jnp.exp(jnp.sum(fading_channel_groups, axis=0))

    def chain_states(earlier, later):
        return (earlier[0] * later[0], later[0][:, :, None] * earlier[1] + later[1])

    identity = (jnp.ones_like(through), jnp.zeros_like(nearby_hidden_vector))
    unused_decay, incoming_state = entering(
        (through, nearby_hidden_vector), "sp", chain_states, identity
    )
    running_sum = jnp.cumsum(fading_channel_groups, axis=0)
    recurrent = local_out + jnp.einsum(
        "fby,bym->fbm",
        query_rows_input * jnp.exp(running_sum),
        incoming_state,
        precision=lax.Precision.HIGHEST,
    )
    gated_out = head_norm(recurrent, recurrence_norm_gain.reshape(head_count, HEAD)) * jax.nn.silu(
        gate_b.astype(jnp.float32).reshape(tokens, head_count, HEAD)
    )
    mixed_b = gated_out.reshape(tokens, head_count * HEAD).astype(jnp.bfloat16)
    summed = lax.psum_scatter(
        (contract_rows(mixed_a, out_a) + contract_rows(mixed_b, out_b)).astype(jnp.bfloat16),
        "tp",
        scatter_dimension=0,
        tiled=True,
    )
    layer_out = summed[None]
    return (layer_out, row_log_total)


def solution(mesh):
    return jax.shard_map(
        on_device,
        mesh=mesh,
        in_specs=(
            P("fs", "sp", None),
            P(),
            P(("sp", "fs"), "tp"),
            P(("sp", "fs"), "tp"),
            P(("sp", "fs"), "tp"),
            P(("sp", "fs"), "tp"),
            P(("sp", "fs"), "tp"),
            P(("sp", "fs"), "tp"),
            P(("sp", "fs"), "tp"),
            P(("sp", "fs"), "tp"),
            P(("sp", "fs"), "tp"),
            P("tp"),
            P("tp"),
            P("tp"),
            P("tp"),
            P("tp"),
            P("fs", "sp", "tp"),
        ),
        out_specs=(P("fs", ("sp", "tp"), None), P("fs", "tp", "sp")),
        check_vma=False,
    )
```

profile of v0, /device:TPU:0, one launch (start us, length us, event | category | flops | bytes accessed | tf_op | source)
XLA Modules:
  0.0 472.7 jit_solution(9286617565874748095)
XLA Ops:
  13.5 40.9 %all-gather.16.cloned.1.call-done = bf16[2048,512]{1,0:T(8,128)(2,1)} async-done(((bf16[128,512]{1,0:T(8,128)(2,1)}), bf16[2048,512]{1,0:T(8,128)(2,1)}) %all-gather.16.cloned.1.call-update) | async-done | bytes 2097168 | tf_op jit(solution)/shard_map/all_gather | solution.py:130
  57.8 38.9 %all-gather.12.cloned.1.call-done = bf16[2048,512]{1,0:T(8,128)(2,1)} async-done(((bf16[128,512]{1,0:T(8,128)(2,1)}), bf16[2048,512]{1,0:T(8,128)(2,1)}) %all-gather.12.cloned.1.call-update) | async-done | bytes 2097168 | tf_op jit(solution)/shard_map/all_gather | solution.py:131
  102.2 36.9 %all-gather.22.cloned.1.call-done = bf16[2048,512]{1,0:T(8,128)(2,1)} async-done(((bf16[128,512]{1,0:T(8,128)(2,1)}), bf16[2048,512]{1,0:T(8,128)(2,1)}) %all-gather.22.cloned.1.call-update) | async-done | bytes 2097168 | tf_op jit(solution)/shard_map/all_gather | solution.py:133
  139.1 3.1 fusion.67
  143.6 37.7 %all-gather.26.cloned.1.call-done = bf16[2048,512]{1,0:T(8,128)(2,1)} async-done(((bf16[128,512]{1,0:T(8,128)(2,1)}), bf16[2048,512]{1,0:T(8,128)(2,1)}) %all-gather.26.cloned.1.call-update) | async-done | bytes 2097168 | tf_op jit(solution)/shard_map/all_gather | solution.py:132
  184.3 39.2 %all-gather.24.cloned.1.call-done = bf16[2048,512]{1,0:T(8,128)(2,1)} async-done(((bf16[128,512]{1,0:T(8,128)(2,1)}), bf16[2048,512]{1,0:T(8,128)(2,1)}) %all-gather.24.cloned.1.call-update) | async-done | bytes 2097168 | tf_op jit(solution)/shard_map/all_gather | solution.py:134
  226.4 24.0 %while.43 = (s32[]{:T(128)}, f32[4,128,128]{2,1,0:T(8,128)S(1)}, f32[4,64,4,128]{3,1,0,2:T(8,128)}, f32[4,64,4,128]{3,2,1,0:T(4,128)S(1)}, f32[4,64,4,128]{3,2,1...) while((s32[]{:T(128)}, f32[4,128,128]{2,1,0:T(8,128)S(1)}, ...), condition=%wide.region_13.14_spmd.clone, body=%wide.region_10.13_spmd.clone.sunk | while | flops 138760192 | bytes 4346484 | solution.py:194
  226.7 3.7 multiply_reduce_fusion.4
  232.7 3.7 multiply_reduce_fusion.4
  238.7 3.7 multiply_reduce_fusion.4
  244.7 3.7 multiply_reduce_fusion.4
  250.5 20.1 %all-gather = bf16[16,128,128]{2,1,0:T(8,128)(2,1)S(1)} all-gather(bf16[4,128,128]{2,1,0:T(8,128)(2,1)S(1)} %convert_element_type.119), channel_id=2, replica_groups=mesh['sp'=4,'fs'=4,'tp'=2] {'sp'}, dimensions={0}, use_global_device_ids=true | all-gather | bytes 655360 | tf_op jit(solution)/shard_map/all_gather | solution.py:15
  270.6 9.2 %all_gather.48 = bf16[4,4,128]{2,1,0:T(4,128)(2,1)S(1)} all-gather(bf16[1,4,128]{2,1,0:T(4,128)(2,1)S(1)} %fusion.58), channel_id=1, replica_groups=mesh['sp'=4,'fs'=4,'tp'=2] {'sp'}, dimensions={0}, use_global_device_ids=true | all-gather | bytes 5120 | tf_op jit(solution)/shard_map/all_gather | solution.py:15
  279.8 12.2 %while.44 = (s32[]{:T(128)}, f32[4,128,128]{2,1,0:T(8,128)S(1)}, s32[]{:T(128)}, bf16[4,4,128]{2,1,0:T(4,128)(2,1)S(1)}, bf16[4,4,128,128]{3,2,1,0:T(8,128)(2,1)S(1)}, /*index=5*/s32[]{:T(128)}, s32[]{:T(128)}) while((s32[]{:T(128)}, f32[4,128,128]{2,1,0:T(8,128)S(1)}, s32[]{:T(128)}, bf16[4,4,128]{2,1,0:T(4,128)(2,1)S(1)}, ...), condition=%wide.region_16.17_spmd.clone, body=%wide.region_15.16_spmd.clone.sunk | while | flops 328196 | bytes 660585 | solution.py:32
  297.3 14.6 %all-gather.14.cloned.1.call-done = bf16[2048,512]{1,0:T(8,128)(2,1)} async-done(((bf16[128,512]{1,0:T(8,128)(2,1)}), bf16[2048,512]{1,0:T(8,128)(2,1)}) %all-gather.14.cloned.1.call-update) | async-done | bytes 2097168 | tf_op jit(solution)/shard_map/all_gather | solution.py:129
  316.2 9.2 %fusion.48 = f32[4,256,2,128]{1,2,3,0:T(2,128)S(1)} fusion(f32[4,256,2,128]{1,3,2,0:T(8,128)S(1)} %bitcast.197), kind=kOutput, calls=%fused_computation.90 | output fusion | flops 33292288 | bytes 2097152 | tf_op jit(solution)/shard_map/reduce-window
  328.6 29.9 %all-gather.18.cloned.1.call-done = bf16[2,1024,4,128]{3,1,2,0:T(8,128)(2,1)} async-done(((bf16[2,256,4,128]{3,1,2,0:T(8,128)(2,1)}), bf16[2,1024,4,128]{3,1,2,0:T(8,128)(2,1)}) %all-gather.18.cloned.1.call-update) | async-done | bytes 2097168 | tf_op jit(solution)/shard_map/all_gather | solution.py:159
  358.5 43.2 %while.42 = (s32[]{:T(128)}, f32[256,4,128]{0,2,1:T(8,128)S(1)}, f32[4,256]{1,0:T(4,128)S(1)}, s32[]{:T(128)}, bf16[2,1024,4,128]{3,1,2,0:T(8,128)(2,1)}, /*inde...) while((s32[]{:T(128)}, f32[256,4,128]{0,2,1:T(8,128)S(1)}, ...), condition=%wide.region_8.9_spmd, body=%wide.region_4.8_spmd.sunk | while | flops 175772672 | bytes 13451514 | solution.py:169
  360.4 9.2 %fusion.108 = f32[4,256,2,128]{1,2,3,0:T(2,128)S(1)} fusion(f32[4,256,2,128]{1,3,2,0:T(8,128)S(1)} %bitcast.196), kind=kOutput, calls=%fused_computation.14.clone.1 | output fusion | flops 33292288 | bytes 2097152 | tf_op jit(solution)/shard_map/reduce-window.8
  374.8 9.2 %fusion.108 = f32[4,256,2,128]{1,2,3,0:T(2,128)S(1)} fusion(f32[4,256,2,128]{1,3,2,0:T(8,128)S(1)} %bitcast.196), kind=kOutput, calls=%fused_computation.14.clone.1 | output fusion | flops 33292288 | bytes 2097152 | tf_op jit(solution)/shard_map/reduce-window.8
  389.2 9.2 %fusion.108 = f32[4,256,2,128]{1,2,3,0:T(2,128)S(1)} fusion(f32[4,256,2,128]{1,3,2,0:T(8,128)S(1)} %bitcast.196), kind=kOutput, calls=%fused_computation.14.clone.1 | output fusion | flops 33292288 | bytes 2097152 | tf_op jit(solution)/shard_map/reduce-window.8
  404.3 38.9 %all-gather.30.cloned.1.call-done = bf16[2048,512]{1,0:T(8,128)(2,1)} async-done(((bf16[128,512]{1,0:T(8,128)(2,1)}), bf16[2048,512]{1,0:T(8,128)(2,1)}) %all-gather.30.cloned.1.call-update) | async-done | bytes 2097168 | tf_op jit(solution)/shard_map/all_gather | solution.py:145
  443.2 3.3 fusion.31
  447.2 18.6 %reduce-scatter.2.cloned.1.call-done = bf16[128,2048]{1,0:T(8,128)(2,1)} async-done(((bf16[256,2048]{1,0:T(8,128)(2,1)}), bf16[128,2048]{1,0:T(8,128)(2,1)}) %reduce-scatter.2.cloned.1.call-update) | async-done | bytes 524304 | tf_op jit(solution)/shard_map/reduce_scatter | solution.py:216
  (189 shorter events, 62.8 us)
Async XLA Ops:
  7.2 47.2 %all-gather.16.cloned.1.call-start = ((), (), s32[]{:S(2)}) async-start(), calls=%async_computation.3 | async-start | bytes 2228224 | tf_op jit(solution)/shard_map/all_gather | solution.py:130
  7.9 88.8 %all-gather.12.cloned.1.call-start = ((), (), s32[]{:S(2)}) async-start(), calls=%async_computation.1 | async-start | bytes 2228224 | tf_op jit(solution)/shard_map/all_gather | solution.py:131
  8.6 130.4 %all-gather.22.cloned.1.call-start = ((), (), s32[]{:S(2)}) async-start(), calls=%async_computation.6 | async-start | bytes 2228224 | tf_op jit(solution)/shard_map/all_gather | solution.py:133
  9.4 171.9 %all-gather.26.cloned.1.call-start = ((), (), s32[]{:S(2)}) async-start(), calls=%async_computation.8 | async-start | bytes 2228224 | tf_op jit(solution)/shard_map/all_gather | solution.py:132
  10.0 213.6 %all-gather.24.cloned.1.call-start = ((), (), s32[]{:S(2)}) async-start(), calls=%async_computation.7 | async-start | bytes 2228224 | tf_op jit(solution)/shard_map/all_gather | solution.py:134
  10.5 284.0 %all-gather.28.cloned.1.call-start = ((), (), s32[]{:S(2)}) async-start(), calls=%async_computation.9 | async-start | bytes 2228224 | tf_op jit(solution)/shard_map/all_gather | solution.py:135
  11.1 300.8 %all-gather.14.cloned.1.call-start = ((), (), s32[]{:S(2)}) async-start(), calls=%async_computation.2 | async-start | bytes 2228224 | tf_op jit(solution)/shard_map/all_gather | solution.py:129
  11.9 346.6 %all-gather.18.cloned.1.call-start = ((), (), s32[]{:S(2)}) async-start(), calls=%async_computation.4 | async-start | bytes 2621440 | tf_op jit(solution)/shard_map/all_gather | solution.py:159
  13.4 83.3 %copy-start.4 = (bf16[1,256,2048]{2,1,0:T(8,128)(2,1)S(1)}, bf16[1,256,2048]{2,1,0:T(8,128)(2,1)}, u32[]{:S(2)}) copy-start(bf16[1,256,2048]{2,1,0:T(8,128)(2,1)} %param.23) | copy-start | bytes 3145732
  13.5 83.3 %copy-start.14 = (f32[2048]{0:T(1024)S(1)}, f32[2048]{0:T(1024)}, u32[]{:S(2)}) copy-start(f32[2048]{0:T(1024)} %param.24) | copy-start | bytes 24580
  99.1 3.1 copy-start.13
  99.1 40.0 %copy-start.15 = (f32[512]{0:T(512)S(1)}, f32[512]{0:T(512)}, u32[]{:S(2)}) copy-start(f32[512]{0:T(512)} %param.38) | copy-start | bytes 6148
  100.1 301.8 %all-gather.20.cloned.1.call-start = ((), (), s32[]{:S(2)}) async-start(), calls=%async_computation.5 | async-start | bytes 2228224 | tf_op jit(solution)/shard_map/all_gather | solution.py:144
  100.8 342.4 %all-gather.30.cloned.1.call-start = ((), (), s32[]{:S(2)}) async-start(), calls=%async_computation.10 | async-start | bytes 2228224 | tf_op jit(solution)/shard_map/all_gather | solution.py:145
  101.4 364.4 %reduce-scatter.2.cloned.1.call-start = ((), (), s32[]{:S(2)}) async-start(), calls=%async_computation.11 | async-start | bytes 1572864 | tf_op jit(solution)/shard_map/reduce_scatter | solution.py:216
  184.1 39.4 %copy-start.2 = (f32[256,512]{1,0:T(8,128)}, f32[256,512]{1,0:T(8,128)S(1)}, u32[]{:S(2)}) copy-start(f32[256,512]{1,0:T(8,128)S(1)} %divide_multiply_fusion) | copy-start | bytes 1572868
  250.5 41.5 %copy-start.8 = (f32[4,64,4,128]{3,1,0,2:T(8,128)S(1)}, f32[4,64,4,128]{3,1,0,2:T(8,128)}, u32[]{:S(2)}) copy-start(f32[4,64,4,128]{3,1,0,2:T(8,128)} %get-tuple-element.260) | copy-start | bytes 1572868
  279.8 12.4 %copy-start = (f32[256,4,128]{2,0,1:T(8,128)S(1)}, f32[256,4,128]{2,0,1:T(8,128)}, u32[]{:S(2)}) copy-start(f32[256,4,128]{2,0,1:T(8,128)} %copy_bitcast_fusion.3) | copy-start | bytes 1572868
  292.8 1.8 copy-start.5
  297.3 17.8 %copy-start.10 = (bf16[256,512]{1,0:T(8,128)(2,1)S(1)}, bf16[256,512]{1,0:T(8,128)(2,1)}, u32[]{:S(2)}) copy-start(bf16[256,512]{1,0:T(8,128)(2,1)} %copy-done.9) | copy-start | bytes 786436
  297.3 17.7 %copy-start.16 = (f32[4]{0:T(128)S(1)}, f32[4]{0:T(128)}, u32[]{:S(2)}) copy-start(f32[4]{0:T(128)} %param.34) | copy-start | bytes 52
  325.9 1.7 copy-start.1
  358.5 43.2 %copy-start.12 = (f32[512]{0:T(512)S(1)}, f32[512]{0:T(512)}, u32[]{:S(2)}) copy-start(f32[512]{0:T(512)} %param.35) | copy-start | bytes 6148
  401.9 41.3 %copy-start.6 = (bf16[256,4,128]{0,2,1:T(8,128)(2,1)S(1)}, bf16[256,4,128]{0,2,1:T(8,128)(2,1)}, u32[]{:S(2)}) copy-start(bf16[256,4,128]{0,2,1:T(8,128)(2,1)} %multiply_convert_fusion) | copy-start | bytes 786436
  (4 other events, 4.6 us)
Sparse Core Ops, SparseCore 0:
  10.1 44.1 all-gather.15
  56.5 40.1 all-gather.11
  98.9 40.1 all-gather.21
  141.1 40.1 all-gather.25
  183.3 40.1 all-gather.23
  225.5 43.2 all-gather.27
  271.0 40.8 all-gather.13
  314.1 44.3 all-gather.17
  360.6 40.3 all-gather.19
  403.0 40.1 all-gather.29
  446.7 19.0 reduce-scatter.1
where the time goes:
time: 480 us; the launch traced here: 473 us
  waiting for transfers between devices  301 us (63%)
  other arithmetic  66.7 us (14%)
  matrix products  43.6 us (9%)
  blocking collectives  29.3 us (6%)
  between operations  14.7 us (3%)
  loops' own time  11.9 us (2%)
    all_gather x1, waiting for transfers between devices, on_device(): lax.all_gather(weights_in[1], ('sp', 'fs'), axis=0, tiled=True)  40.9 us
    all_gather x1, waiting for transfers between devices, on_device(): lax.all_gather(weights_in[5], ('sp', 'fs'), axis=0, tiled=True)  39.2 us
    all_gather x1, waiting for transfers between devices, on_device(): lax.all_gather(emitted_projection_linear_scan, ('sp', 'fs'), axis=0, tile...  38.9 us
    all_gather x1, waiting for transfers between devices, on_device(): lax.all_gather(weights_in[2], ('sp', 'fs'), axis=0, tiled=True)  38.9 us
    all_gather x1, waiting for transfers between devices, on_device(): lax.all_gather(weights_in[3], ('sp', 'fs'), axis=0, tiled=True)  37.7 us
    another operation x10, other arithmetic  37.4 us
    all_gather x1, waiting for transfers between devices, on_device(): lax.all_gather(weights_in[4], ('sp', 'fs'), axis=0, tiled=True)  36.9 us
    all_gather x1, waiting for transfers between devices, on_device(): gathered = lax.all_gather(key_value, 'sp', axis=1, tiled=True)  29.9 us
  transfers between devices with their start and end apart: 11, of which 9 were waited for; matrix products, arithmetic and copies ran while one was open for 23% of the time, Pallas kernels for 0%

commit v1 on v0

--- a/solution.py
+++ b/solution.py
@@ -156,7 +156,12 @@
     )
     position = lax.axis_index("sp")
     seq_devices = lax.axis_size("sp")
-    gathered = lax.all_gather(key_value, "sp", axis=1, tiled=True)
+    ring = [key_value]
+    for hop_ in range(3):
+        ring.append(lax.ppermute(ring[-1], "sp", [(dev, (dev + 1) % 4) for dev in range(4)]))
+    gathered = jnp.roll(
+        jnp.concatenate(ring[::-1], axis=1), (lax.axis_index("sp") + 1) * ring[0].shape[1], axis=1
+    )
 
     def gathered_turn(turn_index, carried_state):
         weighted_now, keep_now = carried_state

time: 480 us -> 453 us (0.944)
  waiting for transfers between devices: 301 us -> 268 us
  local copies, waits for them, and re-layouts: 4.66 us -> 16.5 us
  loops' own time: 11.9 us -> 0.85 us
  other arithmetic: 66.7 us -> 74.4 us
    all_gather x1, waiting for transfers between devices: 38.9 us -> 0.02 us  [on_device(): lax.all_gather(emitted_projection_linear_scan, ('sp', 'fs'), axis=0, tile...]
    all_gather x1 -> x0, waiting for transfers between devices: 29.9 us -> none  [on_device(): gathered = lax.all_gather(key_value, 'sp', axis=1, tiled=True)]
    all_gather x1, waiting for transfers between devices: 14.6 us -> 40.7 us  [on_device(): lax.all_gather(weights_in[0], ('sp', 'fs'), axis=0, tiled=True)]
    ppermute x0 -> x3, waiting for transfers between devices: none -> 24.2 us  [on_device(): lax.ppermute(ring[-1], 'sp', [(dev, (dev + 1) % 4) for dev in range(4)])]
    all_gather x1, waiting for transfers between devices: 37.7 us -> 25.8 us  [on_device(): lax.all_gather(weights_in[3], ('sp', 'fs'), axis=0, tiled=True)]
    another operation x1, loops' own time: 11.4 us -> 0.12 us  [entering(): return lax.fori_loop(0, size, hop, start)]
  transfers between devices with their start and end apart: 11 -> 13, of which waited for: 9 -> 9; matrix products, arithmetic and copies ran while one was open for 23% -> 30% of each run, Pallas kernels for 0% -> 0%
where the time goes in v1:
time: 453 us; the launch traced here: 449 us
  waiting for transfers between devices  268 us (59%)
  other arithmetic  74.4 us (16%)
  matrix products  46 us (10%)
  blocking collectives  25.9 us (6%)
  local copies, waits for them, and re-layouts  16.5 us (4%)
  between operations  15 us (3%)
    all_gather x1, waiting for transfers between devices, on_device(): lax.all_gather(weights_in[0], ('sp', 'fs'), axis=0, tiled=True)  40.7 us
    all_gather x1, waiting for transfers between devices, on_device(): lax.all_gather(weights_in[2], ('sp', 'fs'), axis=0, tiled=True)  39.9 us
    all_gather x1, waiting for transfers between devices, on_device(): lax.all_gather(weights_in[4], ('sp', 'fs'), axis=0, tiled=True)  39.3 us
    all_gather x1, waiting for transfers between devices, on_device(): lax.all_gather(weights_in[5], ('sp', 'fs'), axis=0, tiled=True)  38.5 us
    another operation x10, other arithmetic  37.4 us
    all_gather x1, waiting for transfers between devices, on_device(): lax.all_gather(weights_in[1], ('sp', 'fs'), axis=0, tiled=True)  36.7 us
    all_gather x2, blocking collectives, entering(): lax.all_gather(part.astype(kind), axis)  25.9 us
    all_gather x1, waiting for transfers between devices, on_device(): lax.all_gather(weights_in[3], ('sp', 'fs'), axis=0, tiled=True)  25.8 us
  transfers between devices with their start and end apart: 13, of which 9 were waited for; matrix products, arithmetic and copies ran while one was open for 30% of the time, Pallas kernels for 0%

profile of v1, /device:TPU:0, one launch (start us, length us, event | category | flops | bytes accessed | tf_op | source)
XLA Modules:
  0.0 448.8 jit_solution(475462669756955969)
XLA Ops:
  15.1 39.3 %all-gather.19.cloned.1.call-done = bf16[2048,512]{1,0:T(8,128)(2,1)} async-done(((bf16[128,512]{1,0:T(8,128)(2,1)}), bf16[2048,512]{1,0:T(8,128)(2,1)}) %all-gather.19.cloned.1.call-update) | async-done | bytes 2097168 | tf_op jit(solution)/shard_map/all_gather | solution.py:133
  54.4 3.8 fusion.67
  60.1 36.7 %all-gather.15.cloned.1.call-done = bf16[2048,512]{1,0:T(8,128)(2,1)} async-done(((bf16[128,512]{1,0:T(8,128)(2,1)}), bf16[2048,512]{1,0:T(8,128)(2,1)}) %all-gather.15.cloned.1.call-update) | async-done | bytes 2097168 | tf_op jit(solution)/shard_map/all_gather | solution.py:130
  99.2 39.9 %all-gather.11.cloned.1.call-done = bf16[2048,512]{1,0:T(8,128)(2,1)} async-done(((bf16[128,512]{1,0:T(8,128)(2,1)}), bf16[2048,512]{1,0:T(8,128)(2,1)}) %all-gather.11.cloned.1.call-update) | async-done | bytes 2097168 | tf_op jit(solution)/shard_map/all_gather | solution.py:131
  143.3 40.7 %all-gather.13.cloned.1.call-done = bf16[2048,512]{1,0:T(8,128)(2,1)} async-done(((bf16[128,512]{1,0:T(8,128)(2,1)}), bf16[2048,512]{1,0:T(8,128)(2,1)}) %all-gather.13.cloned.1.call-update) | async-done | bytes 2097168 | tf_op jit(solution)/shard_map/all_gather | solution.py:129
  188.5 9.2 %fusion.48 = f32[4,256,2,128]{1,2,3,0:T(2,128)S(1)} fusion(f32[4,256,2,128]{1,3,2,0:T(8,128)S(1)} %bitcast.197), kind=kOutput, calls=%fused_computation.90 | output fusion | flops 33292288 | bytes 2097152 | tf_op jit(solution)/shard_map/reduce-window
  200.4 25.8 %all-gather.23.cloned.1.call-done = bf16[2048,512]{1,0:T(8,128)(2,1)} async-done(((bf16[128,512]{1,0:T(8,128)(2,1)}), bf16[2048,512]{1,0:T(8,128)(2,1)}) %all-gather.23.cloned.1.call-update) | async-done | bytes 2097168 | tf_op jit(solution)/shard_map/all_gather | solution.py:132
  229.9 38.5 %all-gather.21.cloned.1.call-done = bf16[2048,512]{1,0:T(8,128)(2,1)} async-done(((bf16[128,512]{1,0:T(8,128)(2,1)}), bf16[2048,512]{1,0:T(8,128)(2,1)}) %all-gather.21.cloned.1.call-update) | async-done | bytes 2097168 | tf_op jit(solution)/shard_map/all_gather | solution.py:134
  271.3 31.5 %while.43 = (s32[]{:T(128)}, f32[4,128,128]{2,1,0:T(8,128)S(1)}, f32[4,64,4,128]{3,1,0,2:T(8,128)}, f32[4,64,4,128]{3,2,1,0:T(4,128)}, f32[4,64,4,128]{3,2,1,0:T...) while((s32[]{:T(128)}, f32[4,128,128]{2,1,0:T(8,128)S(1)}, ...), condition=%wide.region_13.14_spmd.clone, body=%wide.region_10.13_spmd.clone.sunk | while | flops 138760192 | bytes 4346992 | solution.py:199
  273.4 3.7 multiply_reduce_fusion.4
  281.3 3.7 multiply_reduce_fusion.4
  289.2 3.7 multiply_reduce_fusion.4
  297.0 3.7 multiply_reduce_fusion.4
  302.8 16.8 %all-gather = bf16[16,128,128]{2,1,0:T(8,128)(2,1)S(1)} all-gather(bf16[4,128,128]{2,1,0:T(8,128)(2,1)S(1)} %convert_element_type.119), channel_id=2, replica_groups=mesh['sp'=4,'fs'=4,'tp'=2] {'sp'}, dimensions={0}, use_global_device_ids=true | all-gather | bytes 655360 | tf_op jit(solution)/shard_map/all_gather | solution.py:15
  319.7 9.1 %all_gather.44 = bf16[4,4,128]{2,1,0:T(4,128)(2,1)S(1)} all-gather(bf16[1,4,128]{2,1,0:T(4,128)(2,1)S(1)} %fusion.58), channel_id=1, replica_groups=mesh['sp'=4,'fs'=4,'tp'=2] {'sp'}, dimensions={0}, use_global_device_ids=true | all-gather | bytes 5120 | tf_op jit(solution)/shard_map/all_gather | solution.py:15
  332.2 3.6 fusion.41
  339.5 19.5 %collective-permute-done.1 = bf16[2,256,4,128]{3,1,2,0:T(8,128)(2,1)S(1)} collective-permute-done((bf16[2,256,4,128]{3,1,2,0:T(8,128)(2,1)}, bf16[2,256,4,128]{3,1,2,0:T(8,128)(2,1)S(1)}, u32[]{:S(2)}, u32[]{:S(2)}) %collective-permute-start.1) | collective-permute-done | bytes 524320 | tf_op jit(solution)/shard_map/ppermute | solution.py:161
  365.2 4.7 %collective-permute-done.2 = bf16[2,256,4,128]{3,1,2,0:T(8,128)(2,1)S(1)} collective-permute-done((bf16[2,256,4,128]{3,1,2,0:T(8,128)(2,1)S(1)}, bf16[2,256,4,128]{3,1,2,0:T(8,128)(2,1)S(1)}, u32[]{:S(2)}, u32[]{:S(2)}) %collective-permute-start.2) | collective-permute-done | bytes 524320 | tf_op jit(solution)/shard_map/ppermute | solution.py:161
  374.3 43.1 %while.42 = (s32[]{:T(128)}, f32[256,4,128]{0,2,1:T(8,128)S(1)}, f32[4,256]{1,0:T(4,128)S(1)}, s32[]{:T(128)}, bf16[2,1024,4,128]{3,1,2,0:T(8,128)(2,1)}, /*inde...) while((s32[]{:T(128)}, f32[256,4,128]{0,2,1:T(8,128)S(1)}, ...), condition=%wide.region_8.9_spmd, body=%wide.region_4.8_spmd.sunk | while | flops 175772672 | bytes 13451514 | solution.py:174
  376.3 9.2 %fusion.108 = f32[4,256,2,128]{1,2,3,0:T(2,128)S(1)} fusion(f32[4,256,2,128]{1,3,2,0:T(8,128)S(1)} %bitcast.196), kind=kOutput, calls=%fused_computation.14.clone.1 | output fusion | flops 33292288 | bytes 2097152 | tf_op jit(solution)/shard_map/reduce-window.8
  390.6 9.2 %fusion.108 = f32[4,256,2,128]{1,2,3,0:T(2,128)S(1)} fusion(f32[4,256,2,128]{1,3,2,0:T(8,128)S(1)} %bitcast.196), kind=kOutput, calls=%fused_computation.14.clone.1 | output fusion | flops 33292288 | bytes 2097152 | tf_op jit(solution)/shard_map/reduce-window.8
  405.0 9.2 %fusion.108 = f32[4,256,2,128]{1,2,3,0:T(2,128)S(1)} fusion(f32[4,256,2,128]{1,3,2,0:T(8,128)S(1)} %bitcast.196), kind=kOutput, calls=%fused_computation.14.clone.1 | output fusion | flops 33292288 | bytes 2097152 | tf_op jit(solution)/shard_map/reduce-window.8
  420.1 3.3 fusion.31
  424.1 17.6 %reduce-scatter.2.cloned.1.call-done = bf16[128,2048]{1,0:T(8,128)(2,1)} async-done(((bf16[256,2048]{1,0:T(8,128)(2,1)}), bf16[128,2048]{1,0:T(8,128)(2,1)}) %reduce-scatter.2.cloned.1.call-update) | async-done | bytes 524304 | tf_op jit(solution)/shard_map/reduce_scatter | solution.py:221
  (223 shorter events, 82.8 us)
Async XLA Ops:
  7.2 47.2 %copy-start.6 = (bf16[1,256,2048]{2,1,0:T(8,128)(2,1)S(1)}, bf16[1,256,2048]{2,1,0:T(8,128)(2,1)}, u32[]{:S(2)}) copy-start(bf16[1,256,2048]{2,1,0:T(8,128)(2,1)} %param.23) | copy-start | bytes 3145732
  7.2 47.2 %copy-start.21 = (f32[2048]{0:T(1024)S(1)}, f32[2048]{0:T(1024)}, u32[]{:S(2)}) copy-start(f32[2048]{0:T(1024)} %param.24) | copy-start | bytes 24580
  7.2 47.2 %copy-start.24 = (f32[512]{0:T(512)S(1)}, f32[512]{0:T(512)}, u32[]{:S(2)}) copy-start(f32[512]{0:T(512)} %param.38) | copy-start | bytes 6148
  7.2 47.2 %copy-start.20 = (f32[1,256,512]{2,1,0:T(8,128)S(1)}, f32[1,256,512]{2,1,0:T(8,128)}, u32[]{:S(2)}) copy-start(f32[1,256,512]{2,1,0:T(8,128)} %param.39) | copy-start | bytes 1572868
  7.2 47.2 %all-gather.19.cloned.1.call-start = ((), (), s32[]{:S(2)}) async-start(), calls=%async_computation.5 | async-start | bytes 2228224 | tf_op jit(solution)/shard_map/all_gather | solution.py:133
  8.0 88.8 %all-gather.15.cloned.1.call-start = ((), (), s32[]{:S(2)}) async-start(), calls=%async_computation.3 | async-start | bytes 2228224 | tf_op jit(solution)/shard_map/all_gather | solution.py:130
  8.7 130.4 %all-gather.11.cloned.1.call-start = ((), (), s32[]{:S(2)}) async-start(), calls=%async_computation.1 | async-start | bytes 2228224 | tf_op jit(solution)/shard_map/all_gather | solution.py:131
  9.4 174.5 %all-gather.13.cloned.1.call-start = ((), (), s32[]{:S(2)}) async-start(), calls=%async_computation.2 | async-start | bytes 2228224 | tf_op jit(solution)/shard_map/all_gather | solution.py:129
  10.0 216.1 %all-gather.23.cloned.1.call-start = ((), (), s32[]{:S(2)}) async-start(), calls=%async_computation.7 | async-start | bytes 2228224 | tf_op jit(solution)/shard_map/all_gather | solution.py:132
  10.6 257.8 %all-gather.21.cloned.1.call-start = ((), (), s32[]{:S(2)}) async-start(), calls=%async_computation.6 | async-start | bytes 2228224 | tf_op jit(solution)/shard_map/all_gather | solution.py:134
  11.2 321.0 %all-gather.25.cloned.1.call-start = ((), (), s32[]{:S(2)}) async-start(), calls=%async_computation.8 | async-start | bytes 2228224 | tf_op jit(solution)/shard_map/all_gather | solution.py:135
  11.9 405.8 %all-gather.17.cloned.1.call-start = ((), (), s32[]{:S(2)}) async-start(), calls=%async_computation.4 | async-start | bytes 2228224 | tf_op jit(solution)/shard_map/all_gather | solution.py:144
  12.7 407.4 %all-gather.27.cloned.1.call-start = ((), (), s32[]{:S(2)}) async-start(), calls=%async_computation.9 | async-start | bytes 2228224 | tf_op jit(solution)/shard_map/all_gather | solution.py:145
  13.4 428.3 %reduce-scatter.2.cloned.1.call-start = ((), (), s32[]{:S(2)}) async-start(), calls=%async_computation.10 | async-start | bytes 1572864 | tf_op jit(solution)/shard_map/reduce_scatter | solution.py:221
  15.1 168.8 %copy-start.17 = (f32[256]{0:T(256)}, f32[256]{0:T(256)S(1)}, u32[]{:S(2)}) copy-start(f32[256]{0:T(256)S(1)} %add_rsqrt_fusion.2) | copy-start | bytes 3076
  99.1 42.4 %copy-start.13 = (bf16[256,512]{1,0:T(8,128)(2,1)}, bf16[256,512]{1,0:T(8,128)(2,1)S(1)}, u32[]{:S(2)}) copy-start(bf16[256,512]{1,0:T(8,128)(2,1)S(1)} %convolution_convert_fusion.4) | copy-start | bytes 786436
  141.5 42.4 %copy-start.7 = (bf16[256,512]{1,0:T(8,128)(2,1)}, bf16[256,512]{1,0:T(8,128)(2,1)S(1)}, u32[]{:S(2)}) copy-start(bf16[256,512]{1,0:T(8,128)(2,1)S(1)} %convolution_convert_fusion.6) | copy-start | bytes 786436
  142.5 43.8 %copy-start.25 = (f32[4]{0:T(128)S(1)}, f32[4]{0:T(128)}, u32[]{:S(2)}) copy-start(f32[4]{0:T(128)} %param.34) | copy-start | bytes 52
  142.5 193.4 %collective-permute-start = (bf16[2,256,4,128]{3,1,2,0:T(8,128)(2,1)}, bf16[2,256,4,128]{3,1,2,0:T(8,128)(2,1)}, u32[]{:S(2)}, u32[]{:S(2)}) collective-permute-start(bf16[2,256,4,128]{3,1,2,0:T(8,128)(2,1)} %pad_maximum_fusion), channel_id=1, source_target_pairs={{0,8},{8,16},{16,24},{24,0},{1,9},{9,17},{17,25},{25,1},{2,10},{10... | collective-permute-start | bytes 1572872 | tf_op jit(solution)/shard_map/ppermute | solution.py:161
  198.1 28.0 %copy-start.18 = (f32[256]{0:T(256)S(1)}, f32[256]{0:T(256)}, u32[]{:S(2)}) copy-start(f32[256]{0:T(256)} %copy-done.17) | copy-start | bytes 3076
  228.9 39.5 %copy-start.2 = (f32[256,512]{1,0:T(8,128)}, f32[256,512]{1,0:T(8,128)S(1)}, u32[]{:S(2)}) copy-start(f32[256,512]{1,0:T(8,128)S(1)} %divide_multiply_fusion) | copy-start | bytes 1572868
  335.8 23.2 %collective-permute-start.1 = (bf16[2,256,4,128]{3,1,2,0:T(8,128)(2,1)}, bf16[2,256,4,128]{3,1,2,0:T(8,128)(2,1)S(1)}, u32[]{:S(2)}, u32[]{:S(2)}) collective-permute-start(bf16[2,256,4,128]{3,1,2,0:T(8,128)(2,1)} %collective-permute-done), channel_id=1, source_target_pairs={{0,8},{8,16},{16,24},{24,0},{1,9},{9,17},{17,25},{25,1},{2,10},{10... | collective-permute-start | bytes 1572872 | tf_op jit(solution)/shard_map/ppermute | solution.py:161
  359.0 11.0 %collective-permute-start.2 = (bf16[2,256,4,128]{3,1,2,0:T(8,128)(2,1)S(1)}, bf16[2,256,4,128]{3,1,2,0:T(8,128)(2,1)S(1)}, u32[]{:S(2)}, u32[]{:S(2)}) collective-permute-start(bf16[2,256,4,128]{3,1,2,0:T(8,128)(2,1)S(1)} %collective-permute-done.1), channel_id=1, source_target_pairs={{0,8},{8,16},{16,24},{24,0},{1,9},{9,17},{17,25},{25,1},{2,10},{10... | collective-permute-start | bytes 1572872 | tf_op jit(solution)/shard_map/ppermute | solution.py:161
  374.3 43.2 %copy-start.15 = (f32[512]{0:T(512)S(1)}, f32[512]{0:T(512)}, u32[]{:S(2)}) copy-start(f32[512]{0:T(512)} %param.35) | copy-start | bytes 6148
  (16 other events, 126.4 us)
Sparse Core Ops, SparseCore 0:
  10.2 44.1 all-gather.18
  56.6 40.1 all-gather.14
  98.9 40.1 all-gather.10
  141.2 42.7 all-gather.12
  185.9 40.1 all-gather.22
  228.2 40.1 all-gather.20
  270.5 41.0 all-gather.24
  313.8 48.9 all-gather.16
  365.0 38.7 all-gather.26
  423.6 18.0 reduce-scatter.1
